TPU v7x, 32 devices: a whole 2x2x4 slice. The times are simulated.
32 devices in a mesh: grp: 2 (over y), kv: 4 (over z), tp: 4 (over x, core).
Axes of the slice: x: 2, y: 2, z: 4, core: 2. Of those that a mesh axis runs over, the one named last changes fastest.
Arguments:
- residual: bfloat16 [32, 4096], P('grp', ('kv', 'tp')), parts along dimension 0, may hold values from -11 to 11
- cache_keys: bfloat16 [32, 4096, 8, 128], P('grp', 'kv', 'tp'), parts along dimension 0, may hold values from -210 to 210
- cache_values: bfloat16 [32, 4096, 8, 128], P('grp', 'kv', 'tp'), parts along dimension 0, may hold values from -6 to 6
- norm_gain: bfloat16 [4096], P('kv'), may hold values from 0.099609375 to 1.8984375
- query_weight: bfloat16 [4096, 2048], P('kv', 'tp'), may hold values from -0.09375 to 0.09375
- key_weight: bfloat16 [4096, 1024], P('kv', 'tp'), may hold values from -0.25 to 0.25
- value_weight: bfloat16 [4096, 1024], P('kv', 'tp'), may hold values from -0.375 to 0.375
- head_lambda: float32 [16], P('tp'), may hold values from 0.3 to 0.8
- head_gain: bfloat16 [128], replicated, may hold values from 0.099609375 to 1.8984375
- out_weight: bfloat16 [2048, 4096], P('tp', 'kv'), may hold values from -0.1875 to 0.1875
- mixer_gain: bfloat16 [4096], P('kv'), may hold values from 0.099609375 to 1.8984375
- up_weight: bfloat16 [4096, 16384], P('kv', 'tp'), may hold values from -0.09375 to 0.09375
- down_weight: bfloat16 [16384, 4096], P('tp', 'kv'), may hold values from -0.0625 to 0.0625
Outputs:
- updated: bfloat16 [32, 4096], P('grp', ('kv', 'tp')), parts along dimension 0
There are 2 independent parts, one for each index of `grp`. A program takes and returns all parts, laid end to end along the dimension named above; an argument that names none is the same for every part. Nothing has to cross between parts.
All inputs are finite; a program needn't handle non-finite values.
Results may differ from a plain program's by a relative error of at most 0.018.
Values may be sent and summed in bfloat16 or wider, within the bound.
A program may use at most 128 MiB of HBM per device.

v0:
```python
import jax
import jax.numpy as jnp
from jax import lax
from jax.sharding import PartitionSpec as P

D = 4096
HEADS = 16
KV_HEADS = 8
HALF = 64
VDIM = 128
EPS = 1e-06


def joined(shard, axis, combine):
    everything = jax.tree.map(lambda part: lax.all_gather(part, axis), shard)
    first = jax.tree.map(lambda part: part[0], everything)

    def step(k, so_far):
        return combine(so_far, jax.tree.map(lambda part: part[k], everything))

    return lax.fori_loop(1, lax.axis_size(axis), step, first)


def combine(first, second):
    top = jnp.maximum(first[0], second[0])
    left = jnp.exp(first[0] - top)
    right = jnp.exp(second[0] - top)
    return (
        top,
        first[1] * left + second[1] * right,
        first[2] * left[..., None] + second[2] * right[..., None],
    )


def body(
    residual,
    cache_keys,
    cache_values,
    norm_gain,
    query_weight,
    key_weight,
    value_weight,
    head_lambda,
    head_gain,
    out_weight,
    mixer_gain,
    up_weight,
    down_weight,
):
    f32 = jnp.float32
    bf16 = jnp.bfloat16
    rows = residual.shape[0]
    kv_local = cache_keys.shape[2]
    group = HEADS // KV_HEADS
    scale = 1.0 / HALF**0.5
    block = lax.all_gather(residual, "tp", axis=1, tiled=True).astype(f32)
    scaled = (block * norm_gain.astype(f32)).astype(bf16)
    q_part = jnp.dot(scaled, query_weight, preferred_element_type=f32)
    k_part = jnp.dot(scaled, key_weight, preferred_element_type=f32)
    v_part = jnp.dot(scaled, value_weight, preferred_element_type=f32)
    sq_part = jnp.sum(block * block, axis=1)
    q_sum, k_sum, v_sum, sq_sum = lax.psum((q_part, k_part, v_part, sq_part), "kv")
    inv_rms = lax.rsqrt(sq_sum / D + EPS)[:, None]
    query = (inv_rms * q_sum).astype(bf16).reshape(rows, kv_local, group, 2, HALF)
    new_key = (inv_rms * k_sum).astype(bf16).reshape(rows, kv_local, 2, HALF)
    new_value = (inv_rms * v_sum).astype(bf16).reshape(rows, kv_local, VDIM)
    positions = cache_keys.shape[1]
    keys = cache_keys.reshape(rows, positions, kv_local, 2, HALF)
    scores = jnp.einsum("bkgch,bpkch->bkgcp", query, keys, preferred_element_type=f32) * scale
    local_top = jnp.max(scores, axis=4)
    expo = jnp.exp(scores - local_top[..., None])
    local_total = jnp.sum(expo, axis=4)
    local_weighted = jnp.einsum(
        "bkgcp,bpkv->bkgcv", expo.astype(bf16), cache_values, preferred_element_type=f32
    )
    cache_top, total, weighted = joined((local_top, local_total, local_weighted), "kv", combine)
    own = jnp.einsum("bkgch,bkch->bkgc", query, new_key, preferred_element_type=f32) * scale
    top = jnp.maximum(cache_top, own)
    old_part = jnp.exp(cache_top - top)
    own_part = jnp.exp(own - top)
    numer = (
        weighted * old_part[..., None]
        + own_part[..., None] * new_value.astype(f32)[:, :, None, None, :]
    )
    attended = numer / (total * old_part + own_part)[..., None]
    lambdas = head_lambda.reshape(kv_local, group)[None, :, :, None]
    diff = attended[:, :, :, 0] - lambdas * attended[:, :, :, 1]
    normed = (
        diff * lax.rsqrt(jnp.mean(diff * diff, axis=3, keepdims=True) + EPS) * head_gain.astype(f32)
    )
    heads_out = normed.astype(bf16).reshape(rows, kv_local * group * VDIM)
    projected = jnp.dot(heads_out, out_weight, preferred_element_type=f32)
    mixed = (
        residual.astype(f32) + lax.psum_scatter(projected, "tp", scatter_dimension=1, tiled=True)
    ).astype(bf16)
    mixed_block = lax.all_gather(mixed, "tp", axis=1, tiled=True).astype(f32)
    scaled2 = (mixed_block * mixer_gain.astype(f32)).astype(bf16)
    up_part = jnp.dot(scaled2, up_weight, preferred_element_type=f32)
    sq_mixed = jnp.sum(mixed_block * mixed_block, axis=1)
    up_share = lax.psum_scatter(up_part, "kv", scatter_dimension=1, tiled=True)
    sq_total = lax.psum(sq_mixed, "kv")
    inv_rms2 = lax.rsqrt(sq_total / D + EPS)[:, None]
    share = jnp.square(jnp.maximum(inv_rms2 * up_share, 0.0)).astype(bf16)
    hidden = lax.all_gather(share, "kv", axis=1, tiled=True)
    down_part = jnp.dot(hidden, down_weight, preferred_element_type=f32)
    return (
        mixed.astype(f32) + lax.psum_scatter(down_part, "tp", scatter_dimension=1, tiled=True)
    ).astype(bf16)


def solution(mesh):
    in_specs = (
        P("grp", ("kv", "tp")),
        P("grp", "kv", "tp", None),
        P("grp", "kv", "tp", None),
        P("kv"),
        P("kv", "tp"),
        P("kv", "tp"),
        P("kv", "tp"),
        P("tp"),
        P(),
        P("tp", "kv"),
        P("kv"),
        P("kv", "tp"),
        P("tp", "kv"),
    )
    out_specs = P("grp", ("kv", "tp"))
    return jax.shard_map(body, mesh=mesh, in_specs=in_specs, out_specs=out_specs, check_vma=False)
```

profile of v0, /device:TPU:0, one launch (start us, length us, event | category | flops | bytes accessed | tf_op | source)
XLA Modules:
  0.0 212.5 jit_solution(997170010051651746)
XLA Ops:
  6.5 0.8 convert_element_type.64
  7.3 6.4 %all_gather.27 = bf16[16,1024]{1,0:T(8,128)(2,1)S(1)} all-gather(bf16[16,256]{1,0:T(8,128)(2,1)} %param.15), channel_id=1, replica_groups=mesh['grp'=2,'kv'=4,'tp'=4] {'tp'}, dimensions={1}, use_global_device_ids=true | all-gather | bytes 40960 | tf_op jit(solution)/shard_map/all_gather | solution.py:56
  13.8 0.7 fusion.10
  14.4 1.8 fusion.19
  16.2 1.8 fusion.17
  18.1 2.1 fusion.21
  20.2 0.0 reduce-scatter.4.cloned.1.call-start
  20.2 0.7 mul.232
  21.0 21.2 %copy.77 = bf16[16,1024,2,128]{1,3,2,0:T(8,128)(2,1)} copy(bf16[16,1024,2,128]{3,2,1,0:T(2,128)(2,1)} %param.16) | data formatting | bytes 16777216 | tf_op args[1]
  42.1 14.4 %all-reduce.3.cloned.1.call-done = (f32[16,512]{1,0:T(8,128)}, f32[16]{0:T(128)}, f32[16,256]{1,0:T(8,128)}, f32[16,256]{1,0:T(8,128)}) async-done(((f32[16,512]{1,0:T(8,128)}, f32[16]{0:T(128)}, f32[16,256]{1,0:T(8,128)}, f32[16,256]{1,0:T(8,128)}), (f32[16,512]{1,0:T(8,128)}, f32[16]{0:T(128)}, f32[16,256]{1,0:T(8,128)}, f32[16,256]{1,0:T(8,128)})) %all-reduce.3.cloned.1.call-update) | async-done | bytes 65616 | tf_op jit(solution)/shard_map/psum | solution.py:62
  56.5 0.7 add_rsqrt_fusion.2
  57.2 0.8 multiply_convert_fusion.2
  58.0 0.8 fusion.29
  58.8 0.1 reshape.43
  58.9 0.1 reshape.60
  59.0 0.2 fusion.23
  59.2 0.1 copy.97
  59.3 4.7 %fusion.35 = (f32[16,2,2,2]{2,3,1,0:T(2,128)S(1)}, f32[16,2,2,2,1024]{4,2,3,1,0:T(2,128)S(1)}) fusion(bf16[16,1024,2,2,64]{1,4,3,2,0:T(8,128)(2,1)} %bitcast.56, bf16[16,2,2,2,64]{4,3,2,1,0:T(2,128)(2,1)S(1)} %reshape.43), kind=kOutput, calls=%fused_computation.55 | convolution fusion | flops 17039232 | bytes 8929792 | tf_op jit(solution)/shard_map/bkgch,bpkch->bkgcp/dot_general | solution.py:69
  64.1 0.3 copy.79
  64.4 0.5 fusion.7
  64.9 4.8 %fusion.3 = f32[16,2,2,2,128]{4,2,3,1,0:T(2,128)S(1)} fusion(bf16[16,1024,2,128,1]{3,2,1,0,4:T(2,128)(2,1)} %bitcast.65, f32[16,2,2,2,1024]{4,2,3,1,0:T(2,128)S(1)} %get-tuple-element.245, f32[16,2,2,2]{2,3,1,0:T(2,128)S(1)} %get-tuple-element.244), kind=kOutput, calls=%fused_computation.8 | convolution fusion | flops 33816576 | bytes 8978944 | tf_op jit(solution)/shard_map/bkgcp,bpkv->bkgcv/dot_general | solution.py:73
  69.7 0.3 copy.80
  70.0 13.6 %all-gather.1 = f32[64,2,2,2]{3,2,1,0:T(2,128)S(1)} all-gather(f32[16,2,2,2]{3,2,1,0:T(2,128)S(1)} %copy.80), channel_id=3, replica_groups=mesh['grp'=2,'kv'=4,'tp'=4] {'kv'}, dimensions={0}, use_global_device_ids=true | all-gather | bytes 2560 | tf_op jit(solution)/shard_map/all_gather | solution.py:15
  83.6 0.2 copy.88
  83.8 0.1 copy.86
  83.9 13.5 %all-gather = f32[64,2,2,2]{3,2,1,0:T(2,128)S(1)} all-gather(f32[16,2,2,2]{3,2,1,0:T(2,128)S(1)} %copy.79), channel_id=2, replica_groups=mesh['grp'=2,'kv'=4,'tp'=4] {'kv'}, dimensions={0}, use_global_device_ids=true | all-gather | bytes 2560 | tf_op jit(solution)/shard_map/all_gather | solution.py:15
  97.3 0.2 copy.87
  97.5 0.1 copy.85
  97.6 13.8 %all-gather.2 = f32[64,2,2,2,128]{4,3,2,1,0:T(2,128)S(1)} all-gather(f32[16,2,2,2,128]{4,3,2,1,0:T(2,128)S(1)} %copy.82), channel_id=4, replica_groups=mesh['grp'=2,'kv'=4,'tp'=4] {'kv'}, dimensions={0}, use_global_device_ids=true | all-gather | bytes 327680 | tf_op jit(solution)/shard_map/all_gather | solution.py:15
  111.4 2.1 while.19
  111.4 0.1 copy.115
  111.5 0.1 copy.116
  111.6 0.4 fusion.49
  112.1 0.1 copy.115
  112.2 0.1 copy.116
  112.3 0.4 fusion.49
  112.8 0.1 copy.115
  112.9 0.1 copy.116
  113.0 0.4 fusion.49
  113.5 0.1 copy.91
  113.6 0.1 copy.89
  113.7 0.1 copy.90
  113.8 0.3 add_divide_fusion
  114.1 0.1 slice_reduce_fusion
  114.3 0.2 multiply_reduce_fusion
  114.5 0.1 copy.93
  114.6 0.1 copy.94
  114.7 0.1 mul.240
  114.8 0.1 mul.233
  114.9 0.9 fusion.26
  115.8 0.0 reduce-scatter.6.cloned.1.call-start
  115.9 19.9 %reduce-scatter.4.cloned.1.call-done = f32[16,256]{1,0:T(8,128)} async-done(((f32[16,1024]{1,0:T(8,128)}), f32[16,256]{1,0:T(8,128)}) %reduce-scatter.4.cloned.1.call-update) | async-done | bytes 16400 | tf_op jit(solution)/shard_map/reduce_scatter | solution.py:94
  135.8 0.7 add_convert_fusion.1
  136.5 5.2 %all_gather.34 = bf16[16,1024]{1,0:T(8,128)(2,1)S(1)} all-gather(bf16[16,256]{1,0:T(8,128)(2,1)S(1)} %add_convert_fusion.1), channel_id=1, replica_groups=mesh['grp'=2,'kv'=4,'tp'=4] {'tp'}, dimensions={1}, use_global_device_ids=true | all-gather | bytes 40960 | tf_op jit(solution)/shard_map/all_gather | solution.py:96
  141.7 5.3 %fusion.14 = f32[16,4096]{1,0:T(8,128)} fusion(bf16[1024,4096]{1,0:T(8,128)(2,1)} %param.26, bf16[16,1024]{1,0:T(8,128)(2,1)S(1)} %all_gather.34, f32[1024]{0:T(1024)S(1)} %convert_element_type.77), kind=kOutput, calls=%fused_computation.26 | convolution fusion | flops 134266880 | bytes 8687616 | tf_op jit(solution)/shard_map/dot_general | solution.py:98
  147.0 0.0 reduce-scatter.8.cloned.1.call-start
  147.1 0.1 fusion.12
  147.2 11.8 %psum.39 = f32[16]{0:T(128)S(1)} all-reduce(f32[16]{0:T(128)S(1)} %fusion.12), channel_id=1, replica_groups=mesh['grp'=2,'kv'=4,'tp'=4] {'kv'}, use_global_device_ids=true, to_apply=%region_12.0 | all-reduce | flops 16 | bytes 128 | tf_op jit(solution)/shard_map/psum | solution.py:101
  159.0 8.2 %reduce-scatter.6.cloned.1.call-done = f32[16,1024]{1,0:T(8,128)} async-done(((f32[16,4096]{1,0:T(8,128)}), f32[16,1024]{1,0:T(8,128)}) %reduce-scatter.6.cloned.1.call-update) | async-done | bytes 65552 | tf_op jit(solution)/shard_map/reduce_scatter | solution.py:100
  167.2 0.9 multiply_convert_fusion
  168.1 13.4 %all_gather.35 = bf16[16,4096]{1,0:T(8,128)(2,1)S(1)} all-gather(bf16[16,1024]{1,0:T(8,128)(2,1)S(1)} %multiply_convert_fusion), channel_id=1, replica_groups=mesh['grp'=2,'kv'=4,'tp'=4] {'kv'}, dimensions={1}, use_global_device_ids=true | all-gather | bytes 163840 | tf_op jit(solution)/shard_map/all_gather | solution.py:104
  181.5 5.2 %fusion.36 = f32[16,1024]{1,0:T(8,128)} fusion(bf16[16,4096]{1,0:T(8,128)(2,1)S(1)} %all_gather.35, bf16[4096,1024]{1,0:T(8,128)(2,1)} %param.27), kind=kOutput, calls=%fused_computation.56 | convolution fusion | flops 134217728 | bytes 8585216 | tf_op jit(solution)/shard_map/dot_general | solution.py:105
  186.7 18.0 %reduce-scatter.8.cloned.1.call-done = f32[16,256]{1,0:T(8,128)} async-done(((f32[16,1024]{1,0:T(8,128)}), f32[16,256]{1,0:T(8,128)}) %reduce-scatter.8.cloned.1.call-update) | async-done | bytes 16400 | tf_op jit(solution)/shard_map/reduce_scatter | solution.py:107
  204.7 1.3 add_convert_fusion
  (29 shorter events, 0.4 us)
Async XLA Ops:
  6.5 108.4 %copy-start = (bf16[512,1024]{1,0:T(8,128)(2,1)S(1)}, bf16[512,1024]{1,0:T(8,128)(2,1)}, u32[]{:S(2)}) copy-start(bf16[512,1024]{1,0:T(8,128)(2,1)} %param.24) | copy-start | bytes 3145732
  6.5 50.0 %all-reduce.3.cloned.1.call-start = ((), (), s32[]{:S(2)}) async-start(), calls=%async_computation.6 | async-start | bytes 132096 | tf_op jit(solution)/shard_map/psum | solution.py:62
  20.2 115.6 %reduce-scatter.4.cloned.1.call-start = ((), (), s32[]{:S(2)}) async-start(), calls=%async_computation.3 | async-start | bytes 81920 | tf_op jit(solution)/shard_map/reduce_scatter | solution.py:94
  64.0 50.9 %copy-start.3 = (bf16[128]{0:T(256)(128)(2,1)S(1)}, bf16[128]{0:T(256)(128)(2,1)}, u32[]{:S(2)}) copy-start(bf16[128]{0:T(256)(128)(2,1)} %param.23) | copy-start | bytes 772
  64.0 51.8 %copy-start.2 = (bf16[1024]{0:T(1024)(128)(2,1)S(1)}, bf16[1024]{0:T(1024)(128)(2,1)}, u32[]{:S(2)}) copy-start(bf16[1024]{0:T(1024)(128)(2,1)} %param.25) | copy-start | bytes 6148
  64.1 71.8 %copy-start.1 = (bf16[16,256]{1,0:T(8,128)(2,1)S(1)}, bf16[16,256]{1,0:T(8,128)(2,1)}, u32[]{:S(2)}) copy-start(bf16[16,256]{1,0:T(8,128)(2,1)} %param.15) | copy-start | bytes 24580
  115.8 51.3 %reduce-scatter.6.cloned.1.call-start = ((), (), s32[]{:S(2)}) async-start(), calls=%async_computation.4 | async-start | bytes 327680 | tf_op jit(solution)/shard_map/reduce_scatter | solution.py:100
  147.0 57.6 %reduce-scatter.8.cloned.1.call-start = ((), (), s32[]{:S(2)}) async-start(), calls=%async_computation.5 | async-start | bytes 81920 | tf_op jit(solution)/shard_map/reduce_scatter | solution.py:107
Sparse Core Ops, SparseCore 0:
  20.3 36.1 all-reduce.2
  115.9 19.8 reduce-scatter.3
  147.1 19.9 reduce-scatter.5
  186.8 17.8 reduce-scatter.7
where the time goes:
time: 214 us; the launch traced here: 213 us
  blocking collectives  77.6 us (36%)
  waiting for transfers between devices  60.5 us (28%)
  matrix products  26.7 us (12%)
  local copies, waits for them, and re-layouts  25 us (12%)
  between operations  13.3 us (6%)
  other arithmetic  9.24 us (4%)
    all_gather x3, blocking collectives, joined(): everything = jax.tree.map(lambda part: lax.all_gather(part, axis), shard)  40.8 us
    unnamed x9, local copies, waits for them, and re-layouts  21.2 us
    reduce_scatter x1, waiting for transfers between devices, body(): lax.psum_scatter(projected, 'tp', scatter_dimension=1, tiled=True)  19.9 us
    reduce_scatter x1, waiting for transfers between devices, body(): lax.psum_scatter(down_part, 'tp', scatter_dimension=1, tiled=True)  18 us
    psum x1, waiting for transfers between devices, body(): lax.psum((q_part, k_part, v_part, sq_part), 'kv')  14.4 us
    all_gather x1, blocking collectives, body(): hidden = lax.all_gather(share, 'kv', axis=1, tiled=True)  13.4 us
    psum x1, blocking collectives, body(): sq_total = lax.psum(sq_mixed, 'kv')  11.8 us
    reduce_scatter x1, waiting for transfers between devices, body(): up_share = lax.psum_scatter(up_part, 'kv', scatter_dimension=1, tiled=True)  8.16 us
  transfers between devices with their start and end apart: 4, of which 4 were waited for; matrix products, arithmetic and copies ran while one was open for 10% of the time, Pallas kernels for 0%

commit v1 on v0

--- a/solution.py
+++ b/solution.py
@@ -101,7 +101,9 @@
     sq_total = lax.psum(sq_mixed, "kv")
     inv_rms2 = lax.rsqrt(sq_total / D + EPS)[:, None]
     share = jnp.square(jnp.maximum(inv_rms2 * up_share, 0.0)).astype(bf16)
-    hidden = lax.all_gather(share, "kv", axis=1, tiled=True)
+    hidden = jnp.concatenate(
+        lax.all_to_all(jnp.stack([share] * lax.axis_size("kv")), "kv", 0, 0), axis=1
+    )
     down_part = jnp.dot(hidden, down_weight, preferred_element_type=f32)
     return (
         mixed.astype(f32) + lax.psum_scatter(down_part, "tp", scatter_dimension=1, tiled=True)

time: 214 us -> 210 us (0.981)
  blocking collectives: 77.6 us -> 72.5 us
    all_gather x1 -> x0, blocking collectives: 13.4 us -> none  [body(): hidden = lax.all_gather(share, 'kv', axis=1, tiled=True)]
    all_to_all x0 -> x1, blocking collectives: none -> 8.31 us  [body(): lax.all_to_all(jnp.stack([share] * lax.axis_size('kv')), 'kv', 0, 0)]
  transfers between devices with their start and end apart: 4 -> 4, of which waited for: 4 -> 4; matrix products, arithmetic and copies ran while one was open for 10% -> 11% of each run, Pallas kernels for 0% -> 0%
where the time goes in v1:
time: 210 us; the launch traced here: 208 us
  blocking collectives  72.5 us (35%)
  waiting for transfers between devices  61.3 us (29%)
  matrix products  26.7 us (13%)
  local copies, waits for them, and re-layouts  25 us (12%)
  between operations  13.3 us (6%)
  other arithmetic  9.24 us (4%)
    all_gather x3, blocking collectives, joined(): everything = jax.tree.map(lambda part: lax.all_gather(part, axis), shard)  40.8 us
    unnamed x9, local copies, waits for them, and re-layouts  21.2 us
    reduce_scatter x1, waiting for transfers between devices, body(): lax.psum_scatter(projected, 'tp', scatter_dimension=1, tiled=True)  19.9 us
    reduce_scatter x1, waiting for transfers between devices, body(): lax.psum_scatter(down_part, 'tp', scatter_dimension=1, tiled=True)  18.7 us
    psum x1, waiting for transfers between devices, body(): lax.psum((q_part, k_part, v_part, sq_part), 'kv')  14.4 us
    psum x1, blocking collectives, body(): sq_total = lax.psum(sq_mixed, 'kv')  11.8 us
    all_to_all x1, blocking collectives, body(): lax.all_to_all(jnp.stack([share] * lax.axis_size('kv')), 'kv', 0, 0)  8.31 us
    reduce_scatter x1, waiting for transfers between devices, body(): up_share = lax.psum_scatter(up_part, 'kv', scatter_dimension=1, tiled=True)  8.16 us
  transfers between devices with their start and end apart: 4, of which 4 were waited for; matrix products, arithmetic and copies ran while one was open for 11% of the time, Pallas kernels for 0%

profile of v1, /device:TPU:0, one launch (start us, length us, event | category | flops | bytes accessed | tf_op | source)
XLA Modules:
  0.0 208.2 jit_solution(15791653069957294733)
XLA Ops:
  6.5 0.8 convert_element_type.64
  7.3 6.4 %all_gather.24 = bf16[16,1024]{1,0:T(8,128)(2,1)S(1)} all-gather(bf16[16,256]{1,0:T(8,128)(2,1)} %param.15), channel_id=1, replica_groups=mesh['grp'=2,'kv'=4,'tp'=4] {'tp'}, dimensions={1}, use_global_device_ids=true | all-gather | bytes 40960 | tf_op jit(solution)/shard_map/all_gather | solution.py:56
  13.8 0.7 fusion.10
  14.4 1.8 fusion.19
  16.2 1.8 fusion.17
  18.1 2.1 %fusion.21 = f32[16,512]{1,0:T(8,128)} fusion(bf16[1024,512]{1,0:T(8,128)(2,1)} %param.19, bf16[16,1024]{1,0:T(8,128)(2,1)S(1)} %all_gather.24, f32[1024]{0:T(1024)S(1)} %convert_element_type.64), kind=kOutput, calls=%fused_computation.33 | convolution fusion | flops 16826368 | bytes 1118208 | tf_op jit(solution)/shard_map/dot_general | solution.py:58
  20.2 0.0 reduce-scatter.4.cloned.1.call-start
  20.2 0.7 mul.232
  21.0 21.2 %copy.79 = bf16[16,1024,2,128]{1,3,2,0:T(8,128)(2,1)} copy(bf16[16,1024,2,128]{3,2,1,0:T(2,128)(2,1)} %param.16) | data formatting | bytes 16777216 | tf_op args[1]
  42.1 14.4 %all-reduce.3.cloned.1.call-done = (f32[16,512]{1,0:T(8,128)}, f32[16]{0:T(128)}, f32[16,256]{1,0:T(8,128)}, f32[16,256]{1,0:T(8,128)}) async-done(((f32[16,512]{1,0:T(8,128)}, f32[16]{0:T(128)}, f32[16,256]{1,0:T(8,128)}, f32[16,256]{1,0:T(8,128)}), (f32[16,512]{1,0:T(8,128)}, f32[16]{0:T(128)}, f32[16,256]{1,0:T(8,128)}, f32[16,256]{1,0:T(8,128)})) %all-reduce.3.cloned.1.call-update) | async-done | bytes 65616 | tf_op jit(solution)/shard_map/psum | solution.py:62
  56.5 0.7 add_rsqrt_fusion.2
  57.2 0.8 multiply_convert_fusion.2
  58.0 0.8 fusion.29
  58.8 0.1 reshape.51
  58.9 0.1 reshape.70
  59.0 0.2 fusion.23
  59.2 0.1 copy.100
  59.3 4.7 %fusion.35 = (f32[16,2,2,2]{2,3,1,0:T(2,128)S(1)}, f32[16,2,2,2,1024]{4,2,3,1,0:T(2,128)S(1)}) fusion(bf16[16,1024,2,2,64]{1,4,3,2,0:T(8,128)(2,1)} %bitcast.59, bf16[16,2,2,2,64]{4,3,2,1,0:T(2,128)(2,1)S(1)} %reshape.51), kind=kOutput, calls=%fused_computation.55 | convolution fusion | flops 17039232 | bytes 8929792 | tf_op jit(solution)/shard_map/bkgch,bpkch->bkgcp/dot_general | solution.py:69
  64.1 0.3 copy.81
  64.4 0.5 fusion.7
  64.9 4.8 %fusion.3 = f32[16,2,2,2,128]{4,2,3,1,0:T(2,128)S(1)} fusion(bf16[16,1024,2,128,1]{3,2,1,0,4:T(2,128)(2,1)} %bitcast.70, f32[16,2,2,2,1024]{4,2,3,1,0:T(2,128)S(1)} %get-tuple-element.245, f32[16,2,2,2]{2,3,1,0:T(2,128)S(1)} %get-tuple-element.244), kind=kOutput, calls=%fused_computation.8 | convolution fusion | flops 33816576 | bytes 8978944 | tf_op jit(solution)/shard_map/bkgcp,bpkv->bkgcv/dot_general | solution.py:73
  69.7 0.3 copy.82
  70.0 13.6 %all-gather.1 = f32[64,2,2,2]{3,2,1,0:T(2,128)S(1)} all-gather(f32[16,2,2,2]{3,2,1,0:T(2,128)S(1)} %copy.82), channel_id=3, replica_groups=mesh['grp'=2,'kv'=4,'tp'=4] {'kv'}, dimensions={0}, use_global_device_ids=true | all-gather | bytes 2560 | tf_op jit(solution)/shard_map/all_gather | solution.py:15
  83.6 0.2 copy.90
  83.8 0.1 copy.88
  83.9 13.5 %all-gather = f32[64,2,2,2]{3,2,1,0:T(2,128)S(1)} all-gather(f32[16,2,2,2]{3,2,1,0:T(2,128)S(1)} %copy.81), channel_id=2, replica_groups=mesh['grp'=2,'kv'=4,'tp'=4] {'kv'}, dimensions={0}, use_global_device_ids=true | all-gather | bytes 2560 | tf_op jit(solution)/shard_map/all_gather | solution.py:15
  97.3 0.2 copy.89
  97.5 0.1 copy.87
  97.6 13.8 %all-gather.2 = f32[64,2,2,2,128]{4,3,2,1,0:T(2,128)S(1)} all-gather(f32[16,2,2,2,128]{4,3,2,1,0:T(2,128)S(1)} %copy.84), channel_id=4, replica_groups=mesh['grp'=2,'kv'=4,'tp'=4] {'kv'}, dimensions={0}, use_global_device_ids=true | all-gather | bytes 327680 | tf_op jit(solution)/shard_map/all_gather | solution.py:15
  111.4 2.1 while.19
  111.4 0.1 copy.119
  111.5 0.1 copy.120
  111.6 0.4 fusion.49
  112.1 0.1 copy.119
  112.2 0.1 copy.120
  112.3 0.4 fusion.49
  112.8 0.1 copy.119
  112.9 0.1 copy.120
  113.0 0.4 fusion.49
  113.5 0.1 copy.93
  113.6 0.1 copy.91
  113.7 0.1 copy.92
  113.8 0.3 add_divide_fusion
  114.1 0.1 slice_reduce_fusion
  114.3 0.2 multiply_reduce_fusion
  114.5 0.1 copy.95
  114.6 0.1 copy.96
  114.7 0.1 mul.240
  114.8 0.1 mul.233
  114.9 0.9 fusion.26
  115.8 0.0 reduce-scatter.6.cloned.1.call-start
  115.9 19.9 %reduce-scatter.4.cloned.1.call-done = f32[16,256]{1,0:T(8,128)} async-done(((f32[16,1024]{1,0:T(8,128)}), f32[16,256]{1,0:T(8,128)}) %reduce-scatter.4.cloned.1.call-update) | async-done | bytes 16400 | tf_op jit(solution)/shard_map/reduce_scatter | solution.py:94
  135.8 0.7 add_convert_fusion.1
  136.5 5.2 %all_gather.31 = bf16[16,1024]{1,0:T(8,128)(2,1)S(1)} all-gather(bf16[16,256]{1,0:T(8,128)(2,1)S(1)} %add_convert_fusion.1), channel_id=1, replica_groups=mesh['grp'=2,'kv'=4,'tp'=4] {'tp'}, dimensions={1}, use_global_device_ids=true | all-gather | bytes 40960 | tf_op jit(solution)/shard_map/all_gather | solution.py:96
  141.7 5.3 %fusion.14 = f32[16,4096]{1,0:T(8,128)} fusion(bf16[1024,4096]{1,0:T(8,128)(2,1)} %param.26, bf16[16,1024]{1,0:T(8,128)(2,1)S(1)} %all_gather.31, f32[1024]{0:T(1024)S(1)} %convert_element_type.77), kind=kOutput, calls=%fused_computation.26 | convolution fusion | flops 134266880 | bytes 8687616 | tf_op jit(solution)/shard_map/dot_general | solution.py:98
  147.0 0.0 reduce-scatter.8.cloned.1.call-start
  147.1 0.1 fusion.12
  147.2 11.8 %psum.39 = f32[16]{0:T(128)S(1)} all-reduce(f32[16]{0:T(128)S(1)} %fusion.12), channel_id=1, replica_groups=mesh['grp'=2,'kv'=4,'tp'=4] {'kv'}, use_global_device_ids=true, to_apply=%region_12.0 | all-reduce | flops 16 | bytes 128 | tf_op jit(solution)/shard_map/psum | solution.py:101
  159.0 8.2 %reduce-scatter.6.cloned.1.call-done = f32[16,1024]{1,0:T(8,128)} async-done(((f32[16,4096]{1,0:T(8,128)}), f32[16,1024]{1,0:T(8,128)}) %reduce-scatter.6.cloned.1.call-update) | async-done | bytes 65552 | tf_op jit(solution)/shard_map/reduce_scatter | solution.py:100
  167.2 0.9 multiply_convert_fusion
  168.1 8.3 %all_to_all.5 = bf16[4,16,1024]{2,1,0:T(8,128)(2,1)S(1)} all-to-all(bf16[4,16,1024]{2,1,0:T(8,128)(2,1)S(1)} %stack.2), channel_id=1, replica_groups=mesh['grp'=2,'kv'=4,'tp'=4] {'kv'}, dimensions={0} | all-to-all | bytes 262144 | tf_op jit(solution)/shard_map/all_to_all | solution.py:105
  176.4 5.2 %fusion.36 = f32[16,1024]{1,0:T(8,128)} fusion(bf16[16,4096]{1,0:T(8,128)(2,1)S(1)} %bitcast.61, bf16[4096,1024]{1,0:T(8,128)(2,1)} %param.27), kind=kOutput, calls=%fused_computation.56 | convolution fusion | flops 134217728 | bytes 8585216 | tf_op jit(solution)/shard_map/dot_general | solution.py:107
  181.6 18.7 %reduce-scatter.8.cloned.1.call-done = f32[16,256]{1,0:T(8,128)} async-done(((f32[16,1024]{1,0:T(8,128)}), f32[16,256]{1,0:T(8,128)}) %reduce-scatter.8.cloned.1.call-update) | async-done | bytes 16400 | tf_op jit(solution)/shard_map/reduce_scatter | solution.py:109
  200.4 1.3 add_convert_fusion
  (31 shorter events, 0.4 us)
Async XLA Ops:
  6.5 108.4 %copy-start = (bf16[512,1024]{1,0:T(8,128)(2,1)S(1)}, bf16[512,1024]{1,0:T(8,128)(2,1)}, u32[]{:S(2)}) copy-start(bf16[512,1024]{1,0:T(8,128)(2,1)} %param.24) | copy-start | bytes 3145732
  6.5 50.0 %all-reduce.3.cloned.1.call-start = ((), (), s32[]{:S(2)}) async-start(), calls=%async_computation.7 | async-start | bytes 132096 | tf_op jit(solution)/shard_map/psum | solution.py:62
  20.2 115.6 %reduce-scatter.4.cloned.1.call-start = ((), (), s32[]{:S(2)}) async-start(), calls=%async_computation.4 | async-start | bytes 81920 | tf_op jit(solution)/shard_map/reduce_scatter | solution.py:94
  64.0 50.9 %copy-start.3 = (bf16[128]{0:T(256)(128)(2,1)S(1)}, bf16[128]{0:T(256)(128)(2,1)}, u32[]{:S(2)}) copy-start(bf16[128]{0:T(256)(128)(2,1)} %param.23) | copy-start | bytes 772
  64.0 51.8 %copy-start.2 = (bf16[1024]{0:T(1024)(128)(2,1)S(1)}, bf16[1024]{0:T(1024)(128)(2,1)}, u32[]{:S(2)}) copy-start(bf16[1024]{0:T(1024)(128)(2,1)} %param.25) | copy-start | bytes 6148
  64.1 71.8 %copy-start.1 = (bf16[16,256]{1,0:T(8,128)(2,1)S(1)}, bf16[16,256]{1,0:T(8,128)(2,1)}, u32[]{:S(2)}) copy-start(bf16[16,256]{1,0:T(8,128)(2,1)} %param.15) | copy-start | bytes 24580
  115.8 51.3 %reduce-scatter.6.cloned.1.call-start = ((), (), s32[]{:S(2)}) async-start(), calls=%async_computation.5 | async-start | bytes 327680 | tf_op jit(solution)/shard_map/reduce_scatter | solution.py:100
  147.0 53.4 %reduce-scatter.8.cloned.1.call-start = ((), (), s32[]{:S(2)}) async-start(), calls=%async_computation.6 | async-start | bytes 81920 | tf_op jit(solution)/shard_map/reduce_scatter | solution.py:109
Sparse Core Ops, SparseCore 0:
  20.3 36.1 all-reduce.2
  115.9 19.8 reduce-scatter.3
  147.1 19.9 reduce-scatter.5
  181.8 18.5 reduce-scatter.7
